TPU v7x, 512 devices: a whole 4x4x16 slice. The times are simulated.
512 devices in a mesh: sp: 16 (over z), fs: 4 (over y), tp: 8 (over x, core).
Axes of the slice: x: 4, y: 4, z: 16, core: 2. Of those that a mesh axis runs over, the one named last changes fastest.
Arguments:
- tokens: bfloat16 [4, 16384, 2048], P('fs', 'sp', 'tp'), may hold values from -8 to 8
- norm_gain: float32 [2048], replicated, may hold values from 0.1 to 1.9
- w_query: bfloat16 [2048, 1024], P(('sp', 'fs'), 'tp'), may hold values from -4 to 4
- w_key: bfloat16 [2048, 512], P(('sp', 'fs'), 'tp'), may hold values from -0.16 to 0.16
- w_value: bfloat16 [2048, 512], P(('sp', 'fs'), 'tp'), may hold values from -0.125 to 0.125
- w_conv_in: bfloat16 [2048, 1024], P(('sp', 'fs'), 'tp'), may hold values from -0.125 to 0.125
- w_conv_b: bfloat16 [2048, 1024], P(('sp', 'fs'), 'tp'), may hold values from -0.125 to 0.125
- w_conv_c: bfloat16 [2048, 1024], P(('sp', 'fs'), 'tp'), may hold values from -0.125 to 0.125
- conv_taps: bfloat16 [3, 1024], P(None, 'tp'), may hold values from -3.5 to 3.5
- sink_logits: float32 [16], P('tp'), may hold values from 1 to 5
- w_attn_out: bfloat16 [1024, 2048], P('tp', ('sp', 'fs')), may hold values from -0.375 to 0.375
- w_conv_out: bfloat16 [1024, 2048], P('tp', ('sp', 'fs')), may hold values from -0.125 to 0.125
Outputs:
- mixed: bfloat16 [4, 16384, 2048], P('fs', ('sp', 'tp'))
All inputs are finite; a program needn't handle non-finite values.
Results may differ from a plain program's by a relative error of at most 0.02.
Values may be sent and summed in bfloat16 or wider, within the bound.
A program may use at most 128 MiB of HBM per device.

v0:
```python
import jax
import jax.numpy as jnp
from jax import lax
from jax.sharding import PartitionSpec as P

HEADS = 16
HEAD = 64
WINDOW = 128


def in_one_piece(arrays, axis, dim, along):
    widths = [a.shape[along] for a in arrays]
    both = jnp.concatenate(arrays, axis=along)
    whole = lax.all_gather(both, axis, axis=dim, tiled=True)
    return tuple(jnp.split(whole, [sum(widths[:k]) for k in range(1, len(widths))], axis=along))


def shifted(block, axis, distance):
    devices = range(lax.axis_size(axis))
    route = [(i - distance, i) for i in devices if i - distance in devices]
    return lax.ppermute(block, axis, route)


def rows_first(arrays, axis, dims):
    turned = [jnp.moveaxis(a, dim, 0) for a, dim in zip(arrays, dims)]
    both = jnp.concatenate([t.reshape(len(t), -1) for t in turned], axis=1)
    whole, at, finished = (lax.all_gather(both, axis, axis=0, tiled=True), 0, [])
    for t, dim in zip(turned, dims):
        share = whole[:, at : at + t[0].size].reshape(-1, *t.shape[1:])
        finished.append(jnp.moveaxis(share, 0, dim))
        at += t[0].size
    return tuple(finished)


def norm_rows(tokens, norm_gain):
    values = tokens.astype(jnp.float32)
    average = jnp.mean(values, axis=-1, keepdims=True)
    centred = values - average
    variance = jnp.mean(centred * centred, axis=-1, keepdims=True)
    return (centred * lax.rsqrt(variance + 1e-05) * norm_gain).astype(jnp.bfloat16)


def attend(queries, keys_values, earlier_rows, sink_logits, head_base, row_base):
    row_total = queries.shape[0]
    kv_cols = keys_values.shape[1] // 2
    kv_here = kv_cols // HEAD
    heads_here = queries.shape[1] // HEAD
    group = heads_here // kv_here
    keys_all = jnp.concatenate([earlier_rows, keys_values], axis=0)
    block_rows = min(512, row_total)
    head_ids = head_base + jnp.arange(heads_here, dtype=jnp.int32)
    slopes = jnp.exp2(-8.0 * (head_ids + 1).astype(jnp.float32) / HEADS).reshape(kv_here, group)[
        :, :, None, None
    ]
    sinks = sink_logits.reshape(kv_here, group)[:, :, None, None]
    row_ids = jnp.arange(block_rows, dtype=jnp.int32)[:, None]
    col_ids = jnp.arange(block_rows + WINDOW, dtype=jnp.int32)[None, :]
    distance = WINDOW + row_ids - col_ids
    outputs = []
    for block in range(row_total // block_rows):
        first_row = block * block_rows
        query_block = queries[first_row : first_row + block_rows].reshape(
            block_rows, kv_here, group, HEAD
        )
        band = keys_all[first_row : first_row + block_rows + WINDOW]
        band_keys = band[:, :kv_cols].reshape(block_rows + WINDOW, kv_here, HEAD)
        band_values = band[:, kv_cols:].reshape(block_rows + WINDOW, kv_here, HEAD)
        scores = jnp.einsum(
            "qkgd,skd->kgqs", query_block, band_keys, preferred_element_type=jnp.float32
        ) * HEAD ** (-0.5)
        scores = scores - slopes * distance.astype(jnp.float32)
        key_place = row_base + first_row - WINDOW + col_ids
        keep = (distance >= 0) & (distance < WINDOW) & (key_place >= 0)
        scores = jnp.where(keep, scores, -jnp.inf)
        highest = jnp.maximum(jnp.max(scores, axis=-1, keepdims=True), sinks)
        raised = jnp.exp(scores - highest)
        denominator = jnp.sum(raised, axis=-1, keepdims=True) + jnp.exp(sinks - highest)
        weights = (raised / denominator).astype(jnp.bfloat16)
        mixed = jnp.einsum(
            "kgqs,skd->qkgd", weights, band_values, preferred_element_type=jnp.float32
        )
        outputs.append(mixed.astype(jnp.bfloat16).reshape(block_rows, heads_here * HEAD))
    return jnp.concatenate(outputs, axis=0)


def on_device(
    tokens,
    norm_gain,
    w_query,
    w_key,
    w_value,
    w_conv_in,
    w_conv_b,
    w_conv_c,
    conv_taps,
    sink_logits,
    w_attn_out,
    w_conv_out,
):
    gathered = lax.all_gather(tokens, "tp", axis=2, tiled=True)[0]
    normed = norm_rows(gathered, norm_gain)
    row_total = normed.shape[0]
    weight_rows = in_one_piece(
        (w_query, w_key, w_value, w_conv_in, w_conv_b, w_conv_c), ("sp", "fs"), 0, 1
    )
    results = tuple(
        (
            jnp.dot(normed, rows_part, preferred_element_type=jnp.float32)
            for rows_part in weight_rows
        )
    )
    queries, keys, values, inner, gate_b, gate_c = tuple(
        (result.astype(jnp.bfloat16) for result in results)
    )
    product = (gate_c.astype(jnp.float32) * inner.astype(jnp.float32)).astype(jnp.bfloat16)
    keys_values = jnp.concatenate([keys, values], axis=1)
    earlier_kv, earlier_product = shifted(
        (keys_values[row_total - WINDOW :], product[row_total - 2 :]), "sp", 1
    )
    heads_here = queries.shape[1] // HEAD
    head_base = lax.axis_index("tp") * heads_here
    row_base = lax.axis_index("sp") * row_total
    attended = attend(queries, keys_values, earlier_kv, sink_logits, head_base, row_base)
    taps = conv_taps.astype(jnp.float32)
    padded = jnp.concatenate([earlier_product, product], axis=0).astype(jnp.float32)
    filtered = (
        taps[0] * padded[0:row_total]
        + taps[1] * padded[1 : row_total + 1]
        + taps[2] * padded[2 : row_total + 2]
    )
    conv_out = (gate_b.astype(jnp.float32) * filtered).astype(jnp.bfloat16)
    attn_columns, conv_columns = rows_first((w_attn_out, w_conv_out), ("sp", "fs"), (1, 1))
    summed = lax.psum_scatter(
        (
            jnp.dot(attended, attn_columns, preferred_element_type=jnp.float32)
            + jnp.dot(conv_out, conv_columns, preferred_element_type=jnp.float32)
        ).astype(jnp.bfloat16),
        "tp",
        scatter_dimension=0,
        tiled=True,
    )
    return summed[None]


def solution(mesh):
    placed = (
        P("fs", "sp", "tp"),
        P(),
        P(("sp", "fs"), "tp"),
        P(("sp", "fs"), "tp"),
        P(("sp", "fs"), "tp"),
        P(("sp", "fs"), "tp"),
        P(("sp", "fs"), "tp"),
        P(("sp", "fs"), "tp"),
        P(None, "tp"),
        P("tp"),
        P("tp", ("sp", "fs")),
        P("tp", ("sp", "fs")),
    )
    return jax.shard_map(
        on_device,
        mesh=mesh,
        in_specs=placed,
        out_specs=P("fs", ("sp", "tp"), None),
        check_vma=False,
    )
```

profile of v0, /device:TPU:8, one launch (start us, length us, event | category | flops | bytes accessed | tf_op | source)
XLA Modules:
  0.0 406.5 jit_solution(2349871307167087293)
XLA Ops:
  6.5 0.7 all-gather.4.cloned.1.call-update
  7.3 1.5 concatenate.18
  8.9 1.3 pad_maximum_fusion.4
  10.3 0.7 convert_element_type.108
  11.0 1.2 fusion.14
  12.2 0.5 fusion.32
  12.7 44.3 %all-gather.4.cloned.1.call-done = bf16[1,1024,2048]{2,1,0:T(8,128)(2,1)} async-done(((bf16[1,1024,256]{2,1,0:T(8,128)(2,1)}), bf16[1,1024,2048]{2,1,0:T(8,128)(2,1)}) %all-gather.4.cloned.1.call-update) | async-done | bytes 4194320 | tf_op jit(solution)/shard_map/all_gather | solution.py:100
  57.0 3.0 convert_reduce_fusion
  60.0 0.5 copy-done.1
  60.5 1.2 fusion.3
  61.7 3.0 fusion.5
  64.7 137.2 %all-gather.6.cloned.1.call-done = bf16[2048,640]{1,0:T(8,128)(2,1)} async-done(((bf16[32,640]{1,0:T(8,128)(2,1)}), bf16[2048,640]{1,0:T(8,128)(2,1)}) %all-gather.6.cloned.1.call-update) | async-done | bytes 2621456 | tf_op jit(solution)/shard_map/all_gather | solution.py:14
  201.9 3.9 convolution_convert_fusion.4
  205.8 2.6 convolution_convert_fusion.5
  208.4 3.7 collective-permute-start
  212.1 1.5 convolution_convert_fusion.3
  213.7 1.2 fusion.21
  214.9 1.3 fusion.20
  216.2 2.4 collective-permute-start.1
  218.7 0.9 fusion.65
  219.5 0.2 collective-permute-done.1
  219.8 0.9 fusion.64
  220.8 0.4 fusion.8
  221.1 0.1 exponential_add_fusion.1
  221.2 0.4 fusion.9
  221.6 0.1 exponential_add_fusion
  221.7 0.6 fusion.28
  222.3 0.6 fusion.25
  222.8 117.6 %all-gather.8.cloned.1.call-done = bf16[2048,256]{1,0:T(8,128)(2,1)} async-done(((bf16[32,256]{1,0:T(8,128)(2,1)}), bf16[2048,256]{1,0:T(8,128)(2,1)}) %all-gather.8.cloned.1.call-update) | async-done | bytes 1048592 | tf_op jit(solution)/shard_map/all_gather | solution.py:27
  340.4 5.6 %fusion.42 = f32[1024,2048]{1,0:T(8,128)} fusion(bf16[2048,256]{1,0:T(8,128)(2,1)} %all-gather.8.cloned.1.call-done, bf16[512,128]{0,1:T(8,128)(2,1)S(1)} %bitcast.77, bf16[512,128]{0,1:T(8,128)(2,1)S(1)} %bitcast.78), kind=kOutput, calls=%fused_computation.54 | convolution fusion | flops 537395200 | bytes 9175040 | tf_op jit(solution)/shard_map/dot_general | solution.py:135
  345.9 11.1 %add_convert_fusion = bf16[1024,2048]{1,0:T(8,128)(2,1)} fusion(f32[1024,2048]{1,0:T(8,128)} %fusion.42, bf16[1024,2048]{1,0:T(8,128)(2,1)} %fusion.5, bf16[2048,256]{1,0:T(8,128)(2,1)} %all-gather.8.cloned.1.call-done, f32[1026,128]{1,0:T(8,128)S(1)} %maximum_convert_fusion, bf16[2048,640]{1,0:T(8,128)(2,1)S(1)} %copy-done.2, f32[128]{0:T(128)S(1)} %get-tuple-element.8, ...), kind=kOutput, calls=%fused_computation.8 | convolution fusion | flops 1079115776 | bytes 19400192 | tf_op jit(solution)/shard_map/dot_general | solution.py:136
  357.1 42.9 %reduce-scatter.2.cloned.1.call-done = bf16[128,2048]{1,0:T(8,128)(2,1)} async-done(((bf16[1024,2048]{1,0:T(8,128)(2,1)}), bf16[128,2048]{1,0:T(8,128)(2,1)}) %reduce-scatter.2.cloned.1.call-update) | async-done | bytes 524304 | tf_op jit(solution)/shard_map/reduce_scatter | solution.py:133
  (30 shorter events, 0.4 us)
Async XLA Ops:
  6.5 50.5 %all-gather.4.cloned.1.call-start = ((), (), s32[]{:S(2)}) async-start(), calls=%async_computation.1 | async-start | bytes 4718592 | tf_op jit(solution)/shard_map/all_gather | solution.py:100
  7.3 194.6 %all-gather.6.cloned.1.call-start = ((), (), s32[]{:S(2)}) async-start(), calls=%async_computation.2 | async-start | bytes 2662400 | tf_op jit(solution)/shard_map/all_gather | solution.py:14
  8.8 331.6 %all-gather.8.cloned.1.call-start = ((), (), s32[]{:S(2)}) async-start(), calls=%async_computation.3 | async-start | bytes 1064960 | tf_op jit(solution)/shard_map/all_gather | solution.py:27
  10.2 389.8 %reduce-scatter.2.cloned.1.call-start = ((), (), s32[]{:S(2)}) async-start(), calls=%async_computation.4 | async-start | bytes 4718592 | tf_op jit(solution)/shard_map/reduce_scatter | solution.py:133
  57.0 3.4 copy-start.1
  60.0 1.7 copy-start.4
  201.9 3.9 copy-start
  205.8 6.3 %copy-start.2 = (bf16[2048,640]{1,0:T(8,128)(2,1)S(1)}, bf16[2048,640]{1,0:T(8,128)(2,1)}, u32[]{:S(2)}) copy-start(bf16[2048,640]{1,0:T(8,128)(2,1)} %all-gather.6.cloned.1.call-done) | copy-start | bytes 7864324
  208.4 11.4 %collective-permute-start = (bf16[128,128]{0,1:T(8,128)(2,1)S(1)}, bf16[128,128]{0,1:T(8,128)(2,1)S(1)}, u32[]{:S(2)}, u32[]{:S(2)}) collective-permute-start(bf16[128,128]{0,1:T(8,128)(2,1)S(1)} %pad_maximum_fusion.3), channel_id=1, source_target_pairs={{0,32},{32,64},{64,96},{96,128},{128,160},{160,192},{192,224},{224... | collective-permute-start | bytes 98312 | tf_op jit(solution)/shard_map/ppermute | solution.py:21
  214.9 3.7 copy-start.3
  216.2 3.5 collective-permute-start.1
  219.5 1.2 copy-start.5
Sparse Core Ops, SparseCore 0:
  9.4 47.5 all-gather.3
  60.0 141.8 all-gather.5
  204.8 135.5 all-gather.7
  357.2 42.6 reduce-scatter.1
where the time goes:
time: 407 us; the launch traced here: 406 us
  waiting for transfers between devices  343 us (84%)
  matrix products  30.1 us (7%)
  between operations  13.3 us (3%)
  other arithmetic  12 us (3%)
  starting transfers between devices  6.25 us (2%)
    all_gather x1, waiting for transfers between devices, in_one_piece(): whole = lax.all_gather(both, axis, axis=dim, tiled=True)  137 us
    all_gather x1, waiting for transfers between devices, rows_first(): lax.all_gather(both, axis, axis=0, tiled=True)  118 us
    all_gather x1, waiting for transfers between devices, on_device(): gathered = lax.all_gather(tokens, 'tp', axis=2, tiled=True)[0]  44.3 us
    reduce_scatter x1, waiting for transfers between devices, on_device(): lax.psum_scatter((jnp.dot(attended, attn_columns, preferred_element_type=...  42.9 us
    dot_general x1, matrix products, on_device(): jnp.dot(conv_out, conv_columns, preferred_element_type=jnp.float32)  11.1 us
    dot_general x5, matrix products, on_device(): jnp.dot(normed, rows_part, preferred_element_type=jnp.float32)  10.5 us
  transfers between devices with their start and end apart: 6, of which 5 were waited for; matrix products, arithmetic and copies ran while one was open for 7% of the time, Pallas kernels for 0%

commit v1 on v0

--- a/solution.py
+++ b/solution.py
@@ -6,6 +6,18 @@
 HEADS = 16
 HEAD = 64
 WINDOW = 128
+
+
+def doubled_up(array, axis, dim):
+    ways, here, step = (lax.axis_size(axis), lax.axis_index(axis), array.shape[dim])
+    line, have = (array, 1)
+    while have < ways:
+        line = jnp.concatenate(
+            [line, lax.ppermute(line, axis, [(d, (d - have) % ways) for d in range(ways)])],
+            axis=dim,
+        )
+        have = 2 * have
+    return jnp.roll(line, here * step, axis=dim)
 
 
 def in_one_piece(arrays, axis, dim, along):
@@ -97,7 +109,7 @@
     w_attn_out,
     w_conv_out,
 ):
-    gathered = lax.all_gather(tokens, "tp", axis=2, tiled=True)[0]
+    gathered = doubled_up(tokens, "tp", 2)[0]
     normed = norm_rows(gathered, norm_gain)
     row_total = normed.shape[0]
     weight_rows = in_one_piece(

time: 407 us -> 360 us (0.88)
  waiting for transfers between devices: 343 us -> 286 us
  starting transfers between devices: 6.25 us -> 14.3 us
    all_gather x1, waiting for transfers between devices: 137 us -> 50.9 us  [in_one_piece(): whole = lax.all_gather(both, axis, axis=dim, tiled=True)]
    ppermute x0 -> x3, waiting for transfers between devices: none -> 74.2 us  [doubled_up(): lax.ppermute(line, axis, [(d, (d - have) % ways) for d in range(ways)])]
    all_gather x1 -> x0, waiting for transfers between devices: 44.3 us -> none  [on_device(): gathered = lax.all_gather(tokens, 'tp', axis=2, tiled=True)[0]]
    ppermute x0 -> x3, starting transfers between devices: none -> 7.97 us  [doubled_up(): lax.ppermute(line, axis, [(d, (d - have) % ways) for d in range(ways)])]
  transfers between devices with their start and end apart: 6 -> 8, of which waited for: 5 -> 6; matrix products, arithmetic and copies ran while one was open for 7% -> 8% of each run, Pallas kernels for 0% -> 0%
where the time goes in v1:
time: 360 us
  waiting for transfers between devices  286 us (79%)
  matrix products  30 us (8%)
  starting transfers between devices  14.3 us (4%)
  between operations  13.5 us (4%)
  other arithmetic  13 us (4%)
  local copies, waits for them, and re-layouts  3.68 us (1%)
    all_gather x1, waiting for transfers between devices, rows_first(): lax.all_gather(both, axis, axis=0, tiled=True)  118 us
    ppermute x3, waiting for transfers between devices, doubled_up(): lax.ppermute(line, axis, [(d, (d - have) % ways) for d in range(ways)])  74.2 us
    all_gather x1, waiting for transfers between devices, in_one_piece(): whole = lax.all_gather(both, axis, axis=dim, tiled=True)  50.9 us
    reduce_scatter x1, waiting for transfers between devices, on_device(): lax.psum_scatter((jnp.dot(attended, attn_columns, preferred_element_type=...  42.9 us
    dot_general x1, matrix products, on_device(): jnp.dot(conv_out, conv_columns, preferred_element_type=jnp.float32)  11.1 us
    dot_general x5, matrix products, on_device(): jnp.dot(normed, rows_part, preferred_element_type=jnp.float32)  10.5 us
    ppermute x3, starting transfers between devices, doubled_up(): lax.ppermute(line, axis, [(d, (d - have) % ways) for d in range(ways)])  7.97 us
  transfers between devices with their start and end apart: 8, of which 6 were waited for; matrix products, arithmetic and copies ran while one was open for 8% of the time, Pallas kernels for 0%

profile of v1, /device:TPU:8, one launch (start us, length us, event | category | flops | bytes accessed | tf_op | source)
XLA Modules:
  0.0 360.1 jit_solution(16152560940642645602)
XLA Ops:
  6.5 1.5 concatenate.35
  8.1 2.2 collective-permute-start
  10.3 7.0 %collective-permute-done = bf16[1,1024,256]{2,1,0:T(8,128)(2,1)S(1)} collective-permute-done((bf16[1,1024,256]{2,1,0:T(8,128)(2,1)}, bf16[1,1024,256]{2,1,0:T(8,128)(2,1)S(1)}, u32[]{:S(2)}, u32[]{:S(2)}) %collective-permute-start) | collective-permute-done | bytes 524320 | tf_op jit(solution)/shard_map/ppermute | solution.py:16
  17.3 1.3 pad_maximum_fusion.1
  18.7 2.9 collective-permute-start.1
  21.5 23.7 %collective-permute-done.1 = bf16[1,1024,512]{2,1,0:T(8,128)(2,1)S(1)} collective-permute-done((bf16[1,1024,512]{2,1,0:T(8,128)(2,1)S(1)}, bf16[1,1024,512]{2,1,0:T(8,128)(2,1)S(1)}, u32[]{:S(2)}, u32[]{:S(2)}) %collective-permute-start.1) | collective-permute-done | bytes 1048608 | tf_op jit(solution)/shard_map/ppermute | solution.py:16
  45.2 2.7 pad_maximum_fusion
  47.9 2.9 collective-permute-start.2
  50.8 0.6 pad_maximum_fusion.6
  51.6 1.1 constant_dynamic-update-slice_fusion.7
  52.8 1.2 fusion.32
  54.0 1.3 fusion.14
  55.5 43.5 %collective-permute-done.2 = bf16[1,1024,1024]{2,1,0:T(8,128)(2,1)S(1)} collective-permute-done((bf16[1,1024,1024]{2,1,0:T(8,128)(2,1)}, bf16[1,1024,1024]{2,1,0:T(8,128)(2,1)S(1)}, u32[]{:S(2)}, u32[]{:S(2)}) %collective-permute-start.2) | collective-permute-done | bytes 2097184 | tf_op jit(solution)/shard_map/ppermute | solution.py:16
  99.8 0.6 convert_reduce_fusion
  100.4 1.2 fusion.3
  101.7 3.0 fusion.5
  104.7 50.9 %all-gather.3.cloned.1.call-done = bf16[2048,640]{1,0:T(8,128)(2,1)} async-done(((bf16[32,640]{1,0:T(8,128)(2,1)}), bf16[2048,640]{1,0:T(8,128)(2,1)}) %all-gather.3.cloned.1.call-update) | async-done | bytes 2621456 | tf_op jit(solution)/shard_map/all_gather | solution.py:26
  155.6 3.7 %fusion.18 = f32[1024,128]{1,0:T(8,128)S(1)} fusion(bf16[1024,2048]{1,0:T(8,128)(2,1)} %fusion.5, bf16[2048,640]{1,0:T(8,128)(2,1)} %all-gather.3.cloned.1.call-done), kind=kOutput, calls=%fused_computation.30 | convolution fusion | flops 537133056 | bytes 5242880 | tf_op jit(solution)/shard_map/dot_general | solution.py:120
  159.3 2.4 fusion.21
  161.7 3.7 %collective-permute-start.4 = (bf16[2,128]{1,0:T(2,128)(2,1)S(1)}, bf16[2,128]{1,0:T(2,128)(2,1)S(1)}, u32[]{:S(2)}, u32[]{:S(2)}) collective-permute-start(bf16[2,128]{1,0:T(2,128)(2,1)S(1)} %slice.77), channel_id=1, source_target_pairs={{0,32},{32,64},{64,96},{96,128},{128,160},{160,192},{192,224},{224... | collective-permute-start | bytes 1544 | tf_op jit(solution)/shard_map/ppermute | solution.py:33
  165.4 1.5 convolution_convert_fusion.4
  166.9 1.4 convolution_convert_fusion.5
  168.3 2.5 collective-permute-start.3
  170.9 1.5 convolution_convert_fusion.3
  172.4 0.9 fusion.65
  173.4 0.9 fusion.64
  175.3 0.6 fusion.28
  175.9 0.6 fusion.25
  176.4 117.6 %all-gather.5.cloned.1.call-done = bf16[2048,256]{1,0:T(8,128)(2,1)} async-done(((bf16[32,256]{1,0:T(8,128)(2,1)}), bf16[2048,256]{1,0:T(8,128)(2,1)}) %all-gather.5.cloned.1.call-update) | async-done | bytes 1048592 | tf_op jit(solution)/shard_map/all_gather | solution.py:39
  294.0 5.5 %fusion.42 = f32[1024,2048]{1,0:T(8,128)} fusion(bf16[2048,256]{1,0:T(8,128)(2,1)} %all-gather.5.cloned.1.call-done, bf16[512,128]{0,1:T(8,128)(2,1)S(1)} %bitcast.77, bf16[512,128]{0,1:T(8,128)(2,1)S(1)} %bitcast.78), kind=kOutput, calls=%fused_computation.56 | convolution fusion | flops 537395200 | bytes 9175040 | tf_op jit(solution)/shard_map/dot_general | solution.py:147
  299.5 11.1 %add_convert_fusion = bf16[1024,2048]{1,0:T(8,128)(2,1)} fusion(f32[1024,2048]{1,0:T(8,128)} %fusion.42, bf16[1024,2048]{1,0:T(8,128)(2,1)} %fusion.5, bf16[2048,256]{1,0:T(8,128)(2,1)} %all-gather.5.cloned.1.call-done, f32[1026,128]{1,0:T(8,128)S(1)} %maximum_convert_fusion, bf16[2048,640]{1,0:T(8,128)(2,1)S(1)} %copy-done.4, f32[128]{0:T(128)S(1)} %get-tuple-element.8, ...), kind=kOutput, calls=%fused_computation.8 | convolution fusion | flops 1079115776 | bytes 19400192 | tf_op jit(solution)/shard_map/dot_general | solution.py:148
  310.7 42.9 %reduce-scatter.2.cloned.1.call-done = bf16[128,2048]{1,0:T(8,128)(2,1)} async-done(((bf16[1024,2048]{1,0:T(8,128)(2,1)}), bf16[128,2048]{1,0:T(8,128)(2,1)}) %reduce-scatter.2.cloned.1.call-update) | async-done | bytes 524304 | tf_op jit(solution)/shard_map/reduce_scatter | solution.py:145
  (55 shorter events, 2.3 us)
Async XLA Ops:
  6.5 149.0 %all-gather.3.cloned.1.call-start = ((), (), s32[]{:S(2)}) async-start(), calls=%async_computation.1 | async-start | bytes 2662400 | tf_op jit(solution)/shard_map/all_gather | solution.py:26
  8.0 286.0 %all-gather.5.cloned.1.call-start = ((), (), s32[]{:S(2)}) async-start(), calls=%async_computation.2 | async-start | bytes 1064960 | tf_op jit(solution)/shard_map/all_gather | solution.py:39
  8.1 9.2 %collective-permute-start = (bf16[1,1024,256]{2,1,0:T(8,128)(2,1)}, bf16[1,1024,256]{2,1,0:T(8,128)(2,1)S(1)}, u32[]{:S(2)}, u32[]{:S(2)}) collective-permute-start(bf16[1,1024,256]{2,1,0:T(8,128)(2,1)} %param.12), channel_id=1, source_target_pairs={{0,7},{1,0},{2,1},{3,2},{4,3},{5,4},{6,5},{7,6},{8,15},{9,8},{10,9... | collective-permute-start | bytes 1572872 | tf_op jit(solution)/shard_map/ppermute | solution.py:16
  17.3 30.6 %copy-start.2 = (bf16[1,1024,256]{2,1,0:T(8,128)(2,1)}, bf16[1,1024,256]{2,1,0:T(8,128)(2,1)S(1)}, u32[]{:S(2)}) copy-start(bf16[1,1024,256]{2,1,0:T(8,128)(2,1)S(1)} %collective-permute-done) | copy-start | bytes 1572868
  18.6 32.2 %copy-start.7 = (bf16[128,32]{0,1:T(8,128)(2,1)S(1)}, bf16[128,32]{0,1:T(8,128)(2,1)}, u32[]{:S(2)}) copy-start(bf16[128,32]{0,1:T(8,128)(2,1)} %param.23) | copy-start | bytes 24580
  18.6 32.2 %copy-start.8 = (bf16[128,32]{0,1:T(8,128)(2,1)S(1)}, bf16[128,32]{0,1:T(8,128)(2,1)}, u32[]{:S(2)}) copy-start(bf16[128,32]{0,1:T(8,128)(2,1)} %param.22) | copy-start | bytes 24580
  18.6 32.9 %copy-start.11 = (bf16[3,128]{1,0:T(4,128)(2,1)S(1)}, bf16[3,128]{1,0:T(4,128)(2,1)}, u32[]{:S(2)}) copy-start(bf16[3,128]{1,0:T(4,128)(2,1)} %param.20) | copy-start | bytes 2308
  18.7 26.6 %collective-permute-start.1 = (bf16[1,1024,512]{2,1,0:T(8,128)(2,1)S(1)}, bf16[1,1024,512]{2,1,0:T(8,128)(2,1)S(1)}, u32[]{:S(2)}, u32[]{:S(2)}) collective-permute-start(bf16[1,1024,512]{2,1,0:T(8,128)(2,1)S(1)} %pad_maximum_fusion.1), channel_id=1, source_target_pairs={{0,6},{1,7},{2,0},{3,1},{4,2},{5,3},{6,4},{7,5},{8,14},{9,15},{10,... | collective-permute-start | bytes 3145736 | tf_op jit(solution)/shard_map/ppermute | solution.py:16
  47.9 51.1 %collective-permute-start.2 = (bf16[1,1024,1024]{2,1,0:T(8,128)(2,1)}, bf16[1,1024,1024]{2,1,0:T(8,128)(2,1)S(1)}, u32[]{:S(2)}, u32[]{:S(2)}) collective-permute-start(bf16[1,1024,1024]{2,1,0:T(8,128)(2,1)} %pad_maximum_fusion), channel_id=1, source_target_pairs={{0,4},{1,5},{2,6},{3,7},{4,0},{5,1},{6,2},{7,3},{8,12},{9,13},{10,... | collective-permute-start | bytes 6291464 | tf_op jit(solution)/shard_map/ppermute | solution.py:16
  51.4 302.1 %reduce-scatter.2.cloned.1.call-start = ((), (), s32[]{:S(2)}) async-start(), calls=%async_computation.3 | async-start | bytes 4718592 | tf_op jit(solution)/shard_map/reduce_scatter | solution.py:145
  51.5 3.7 %copy-start.3 = (bf16[1,1024,256]{2,1,0:T(8,128)(2,1)S(1)}, bf16[1,1024,256]{2,1,0:T(8,128)(2,1)}, u32[]{:S(2)}) copy-start(bf16[1,1024,256]{2,1,0:T(8,128)(2,1)} %copy-done.2) | copy-start | bytes 1572868
  55.3 43.9 %copy-start.1 = (bf16[1,1024,256]{2,1,0:T(8,128)(2,1)S(1)}, bf16[1,1024,256]{2,1,0:T(8,128)(2,1)}, u32[]{:S(2)}) copy-start(bf16[1,1024,256]{2,1,0:T(8,128)(2,1)} %param.12) | copy-start | bytes 1572868
  100.4 1.3 copy-start.9
  155.6 3.7 %copy-start = (bf16[1024,2048]{1,0:T(8,128)(2,1)S(1)}, bf16[1024,2048]{1,0:T(8,128)(2,1)}, u32[]{:S(2)}) copy-start(bf16[1024,2048]{1,0:T(8,128)(2,1)} %fusion.5) | copy-start | bytes 12582916
  159.3 6.1 %copy-start.4 = (bf16[2048,640]{1,0:T(8,128)(2,1)S(1)}, bf16[2048,640]{1,0:T(8,128)(2,1)}, u32[]{:S(2)}) copy-start(bf16[2048,640]{1,0:T(8,128)(2,1)} %all-gather.3.cloned.1.call-done) | copy-start | bytes 7864324
  161.7 11.6 %collective-permute-start.4 = (bf16[2,128]{1,0:T(2,128)(2,1)S(1)}, bf16[2,128]{1,0:T(2,128)(2,1)S(1)}, u32[]{:S(2)}, u32[]{:S(2)}) collective-permute-start(bf16[2,128]{1,0:T(2,128)(2,1)S(1)} %slice.77), channel_id=1, source_target_pairs={{0,32},{32,64},{64,96},{96,128},{128,160},{160,192},{192,224},{224... | collective-permute-start | bytes 1544 | tf_op jit(solution)/shard_map/ppermute | solution.py:33
  168.3 4.1 %copy-start.5 = (f32[512,640]{0,1:T(8,128)S(1)}, f32[512,640]{0,1:T(8,128)}, u32[]{:S(2)}) copy-start(f32[512,640]{0,1:T(8,128)} %fusion.14) | copy-start | bytes 3932164
  168.3 4.1 %copy-start.6 = (pred[512,640]{0,1:T(8,128)(4,1)S(1)}, pred[512,640]{0,1:T(8,128)(4,1)}, u32[]{:S(2)}) copy-start(pred[512,640]{0,1:T(8,128)(4,1)} %get-tuple-element.11) | copy-start | bytes 983044
  168.3 5.1 %collective-permute-start.3 = (bf16[128,128]{0,1:T(8,128)(2,1)S(1)}, bf16[128,128]{0,1:T(8,128)(2,1)S(1)}, u32[]{:S(2)}, u32[]{:S(2)}) collective-permute-start(bf16[128,128]{0,1:T(8,128)(2,1)S(1)} %pad_maximum_fusion.5), channel_id=1, source_target_pairs={{0,32},{32,64},{64,96},{96,128},{128,160},{160,192},{192,224},{224... | collective-permute-start | bytes 98312 | tf_op jit(solution)/shard_map/ppermute | solution.py:33
  173.3 1.0 copy-start.10
Sparse Core Ops, SparseCore 0:
  10.3 145.2 all-gather.2
  158.5 135.4 all-gather.4
  310.8 42.6 reduce-scatter.1
